TPU v7x, 256 devices: a whole 4x4x8 slice. The times are simulated.
256 devices in a mesh: ep: 64 (over z, y, core), tp: 4 (over x).
Axes of the slice: x: 4, y: 4, z: 8, core: 2. Of those that a mesh axis runs over, the one named last changes fastest.
Arguments:
- cell_query_rows: bfloat16 [16384, 2048], P('ep', 'tp'), may hold values from -6 to 6
- cell_key_rows: bfloat16 [16384, 2048], P('ep', 'tp'), may hold values from -6 to 6
- cell_value_rows: bfloat16 [16384, 2048], P('ep', 'tp'), may hold values from -6 to 6
- output_gate_logits: bfloat16 [16384, 2048], P('ep', 'tp'), may hold values from -8 to 8
- log_input_gate: float32 [8, 16384], P('tp', 'ep'), may hold values from -4 to 110
- forget_gate_logits: float32 [8, 16384], P('tp', 'ep'), may hold values from -1 to 25
- extra_log_forget: float32 [8, 16384], P('tp', 'ep'), may hold values from -0.7 to 0
- cell_output_scale: float32 [2048], P('tp'), may hold values from 0.1 to 1.9
- tokens_into_experts: bfloat16 [32768, 2048], P(('ep', 'tp')), may hold values from -6 to 6
- expert_norm_scale: float32 [2048], replicated, may hold values from 0.1 to 1.9
- token_expert_index: int32 [32768, 2], P(('ep', 'tp')), may hold values from 0 to 63, all different within a row; in each aligned block of 128 rows (0 to 127, 128 to 255, ...) at most 5 rows name the same one
- chosen_expert_weight: float32 [32768, 2], P(('ep', 'tp')), may hold values from 0.3 to 3
- expert_gate_weight: bfloat16 [64, 2048, 3584], P('ep', None, 'tp'), may hold values from -0.125 to 0.125
- expert_up_weight: bfloat16 [64, 2048, 3584], P('ep', None, 'tp'), may hold values from -0.125 to 0.125
- expert_down_weight: bfloat16 [64, 3584, 2048], P('ep', 'tp'), may hold values from -0.09375 to 0.09375
Outputs:
- gated_head_output: bfloat16 [16384, 2048], P('ep', 'tp')
- expert_output: bfloat16 [32768, 2048], P(('ep', 'tp'))
Inputs may be any that keep to these rules, and one draw needn't show every extreme that they name: `token_expert_index`: each row names 2 different experts. Among the rows of one device (aligned blocks of 128 rows) no expert is named by more than 5 rows, and in every draw some expert is named by exactly 5 rows of some device.
All inputs are finite; a program needn't handle non-finite values.
Results may differ from a plain program's by a relative error of at most 0.012.
Values may be sent and summed in bfloat16 or wider, within the bound.
No kernel may reach another device: no remote copies, remote signals or barrier semaphores. Data moves between devices by JAX's collectives and lax.ppermute only.
A program may use at most 128 MiB of HBM per device.

v0:
```python
import jax
import jax.numpy as jnp
from jax import lax
from jax.sharding import Mesh
from jax.sharding import PartitionSpec as P

HEAD_DIM = 256
BLOCK = 64
TOPK = 2
EP = ("ep_0", "ep_1", "ep_2")
EP_TP = ("ep_0", "ep_1", "ep_2", "tp")
EPSILON = 1e-06
PRECISE = lax.Precision.HIGHEST


def nothing_yet(x, identity):
    return jax.tree.map(
        lambda part, zero: jnp.zeros_like(part) + jnp.asarray(zero, part.dtype), x, identity
    )


def collected_together(x, axis):
    leaves = jax.tree.leaves(x)
    turns = sorted(range(len(leaves)), key=lambda k: -leaves[k].size)
    width = (1, *leaves[turns[0]].shape)[-1]
    lines = [
        jnp.pad(leaves[k].reshape(-1), (0, -leaves[k].size % width)).reshape(-1, width)
        for k in turns
    ]
    both, at, found = (lax.all_gather(jnp.concatenate(lines), axis), 0, {})
    for k, line in zip(turns, lines):
        share = both[:, at : at + len(line)].reshape(len(both), -1)
        found[k] = share[:, : leaves[k].size].reshape(-1, *leaves[k].shape)
        at += len(line)
    numbers = iter(range(len(leaves)))
    return jax.tree.map(lambda _: found[next(numbers)], x)


def entering(x, axes, combine, identity):
    before = start = nothing_yet(x, identity)
    so_far = x
    for axis in reversed(axes):
        size, here = (lax.axis_size(axis), lax.axis_index(axis))
        pieces = collected_together(so_far, axis)
        inside, so_far = (start, start)
        for k in range(size):
            passed = k < here
            so_far = combine(so_far, jax.tree.map(lambda part: part[k], pieces))
            inside = jax.tree.map(lambda new, old: jnp.where(passed, new, old), so_far, inside)
        before = combine(inside, before)
    return before


def split_up(x, dim, size):
    before, after = (x.shape[:dim], x.shape[dim + 1 :])
    return jnp.moveaxis(x.reshape(*before, size, -1, *after), dim, 0)


def sum_at_owner(x, axis, dim):
    size = lax.axis_size(axis)
    blocks = lax.all_to_all(split_up(x, dim, size), axis, 0, 0, tiled=True)
    return jnp.sum(blocks.astype(jnp.float32), axis=0)


def combine(earlier, later):
    cell_early, norm_early, stab_early, total_early = earlier
    cell_late, norm_late, stab_late, total_late = later
    stabilizer = jnp.maximum(total_late + stab_early, stab_late)
    keep_factor = jnp.exp(total_late + stab_early - stabilizer)
    take_factor = jnp.exp(stab_late - stabilizer)
    cell_state = (
        keep_factor[..., None, None] * cell_early + take_factor[..., None, None] * cell_late
    )
    norm_state = keep_factor[..., None] * norm_early + take_factor[..., None] * norm_late
    return (cell_state, norm_state, stabilizer, total_early + total_late)


def mix_heads(
    cell_query_rows,
    cell_key_rows,
    cell_value_rows,
    output_gate_logits,
    log_input_gate,
    forget_gate_logits,
    extra_log_forget,
    cell_output_scale,
):
    n_tok, row_width = cell_query_rows.shape
    head_count = row_width // HEAD_DIM
    block_count = n_tok // BLOCK
    key_scale = HEAD_DIM ** (-0.5)
    block_shape = (block_count, BLOCK, head_count, HEAD_DIM)
    query_blocks = cell_query_rows.reshape(block_shape)
    key_blocks = cell_key_rows.reshape(block_shape)
    value_blocks = cell_value_rows.reshape(block_shape)
    gate_input = log_input_gate.reshape(head_count, block_count, BLOCK)
    forget_gate_value = (jax.nn.log_sigmoid(forget_gate_logits) + extra_log_forget).reshape(
        head_count, block_count, BLOCK
    )
    cumulative = jnp.cumsum(forget_gate_value, axis=-1)
    block_last = cumulative[..., -1]
    growth = block_last[..., None] - cumulative + gate_input
    block_top = jnp.max(growth, axis=-1)
    shares = jnp.exp(growth - block_top[..., None])
    key_float = key_blocks.astype(jnp.float32) * key_scale
    value_weighted = value_blocks.astype(jnp.float32) * shares.transpose(1, 2, 0)[..., None]
    cell_terms = jnp.einsum("bshv,bshk->bhvk", value_weighted, key_float, precision=PRECISE)
    norm_terms = jnp.einsum("hbs,bshk->bhk", shares, key_float, precision=PRECISE)
    block_terms = (cell_terms, norm_terms, block_top.T, block_last.T)
    identity_state = (
        jnp.zeros((head_count, HEAD_DIM, HEAD_DIM), jnp.float32),
        jnp.zeros((head_count, HEAD_DIM), jnp.float32),
        jnp.full((head_count,), -1e30, jnp.float32),
        jnp.zeros((head_count,), jnp.float32),
    )

    def fold_step(running, block_term):
        return (combine(running, block_term), running)

    device_total, before = lax.scan(fold_step, identity_state, block_terms)
    prior_state = entering(device_total, EP, combine, identity_state)
    zero_state = (
        jnp.zeros((head_count, HEAD_DIM, HEAD_DIM), jnp.float32),
        jnp.zeros((head_count, HEAD_DIM), jnp.float32),
        jnp.zeros((head_count,), jnp.float32),
        jnp.zeros((head_count,), jnp.float32),
    )
    start_state = combine(zero_state, prior_state)
    cell_state, norm_state, stabilizer, _ = combine(start_state, before)
    inter_log = cumulative + stabilizer.T[:, :, None]
    causal = jnp.tril(jnp.ones((BLOCK, BLOCK), dtype=bool))
    spread = jnp.where(
        causal,
        cumulative[..., :, None] - cumulative[..., None, :] + gate_input[..., None, :],
        -jnp.inf,
    )
    row_top = jnp.maximum(inter_log, jnp.max(spread, axis=-1))
    intra_weight = jnp.exp(spread - row_top[..., None])
    inter_weight = jnp.exp(inter_log - row_top)
    scores = (
        jnp.einsum("bthd,bshd->hbts", query_blocks, key_blocks, preferred_element_type=jnp.float32)
        * key_scale
        * intra_weight
    )
    weights = scores.astype(jnp.bfloat16)
    numerator = jnp.einsum(
        "hbts,bshd->hbtd", weights, value_blocks, preferred_element_type=jnp.float32
    )
    query_float = query_blocks.astype(jnp.float32)
    numerator = numerator + inter_weight[..., None] * jnp.einsum(
        "bhvk,bthk->hbtv", cell_state, query_float, precision=PRECISE
    )
    denominator = jnp.sum(scores, axis=-1) + inter_weight * jnp.einsum(
        "bhk,bthk->hbt", norm_state, query_float, precision=PRECISE
    )
    cell_out = numerator / jnp.maximum(jnp.abs(denominator), 1.0)[..., None]
    cell_out = cell_out.transpose(1, 2, 0, 3).reshape(n_tok, row_width)
    return (
        cell_out * cell_output_scale * jax.nn.sigmoid(output_gate_logits.astype(jnp.float32))
    ).astype(jnp.bfloat16)


def slot_tables(ids, experts, capacity):
    flat_ids = ids.reshape(-1)
    onehot = (flat_ids[:, None] == jnp.arange(experts, dtype=jnp.int32)[None, :]).astype(jnp.int32)
    earlier = jnp.cumsum(onehot, axis=0) - onehot
    rank_in = jnp.sum(earlier * onehot, axis=1)
    slot_index = flat_ids * capacity + rank_in
    token_of = jnp.arange(flat_ids.shape[0], dtype=jnp.int32) // ids.shape[1]
    slot_hit = slot_index[:, None] == jnp.arange(experts * capacity, dtype=jnp.int32)[None, :]
    slot_owner = jnp.sum(jnp.where(slot_hit, token_of[:, None] + 1, 0), axis=0)
    return (slot_owner, slot_index.reshape(ids.shape))


def local(
    cell_query_rows,
    cell_key_rows,
    cell_value_rows,
    output_gate_logits,
    log_input_gate,
    forget_gate_logits,
    extra_log_forget,
    cell_output_scale,
    tokens_into_experts,
    expert_norm_scale,
    token_expert_index,
    chosen_expert_weight,
    expert_gate_weight,
    expert_up_weight,
    expert_down_weight,
):
    gated_head_output = mix_heads(
        cell_query_rows,
        cell_key_rows,
        cell_value_rows,
        output_gate_logits,
        log_input_gate,
        forget_gate_logits,
        extra_log_forget,
        cell_output_scale,
    )
    ep_count = lax.axis_size(EP)
    n_tok = tokens_into_experts.shape[0]
    experts = ep_count * expert_gate_weight.shape[0]
    capacity = n_tok * TOPK * 5 // (4 * experts)
    input_float = tokens_into_experts.astype(jnp.float32)
    normed = (
        input_float
        * lax.rsqrt(jnp.mean(input_float * input_float, axis=-1, keepdims=True) + EPSILON)
        * expert_norm_scale
    ).astype(jnp.bfloat16)
    gate_matrix = expert_gate_weight[0]
    up_matrix = expert_up_weight[0]
    down_matrix = expert_down_weight[0]
    slot_owner, slot_index = slot_tables(token_expert_index, experts, capacity)
    sendbuf = jnp.where(
        (slot_owner > 0)[:, None],
        normed[jnp.maximum(slot_owner - 1, 0)],
        jnp.zeros((), jnp.bfloat16),
    )
    arrived = lax.all_to_all(sendbuf, EP, split_axis=0, concat_axis=0, tiled=True)
    routed_rows = lax.all_gather(arrived, "tp", axis=0, tiled=True)
    gate_out = jnp.dot(routed_rows, gate_matrix, preferred_element_type=jnp.float32)
    up_out = jnp.dot(routed_rows, up_matrix, preferred_element_type=jnp.float32)
    hidden = (jax.nn.silu(gate_out) * up_out).astype(jnp.bfloat16)
    summed = sum_at_owner(
        jnp.dot(hidden, down_matrix, preferred_element_type=jnp.float32).astype(jnp.bfloat16),
        "tp",
        0,
    ).astype(jnp.bfloat16)
    returned = lax.all_to_all(summed, EP, split_axis=0, concat_axis=0, tiled=True)
    picked = returned[slot_index]
    expert_output = jnp.sum(
        chosen_expert_weight[..., None] * picked.astype(jnp.float32), axis=1
    ).astype(jnp.bfloat16)
    return (gated_head_output, expert_output)


def solution(mesh):
    finer = Mesh(mesh.devices.reshape(8, 4, 2, mesh.shape["tp"]), ("ep_0", "ep_1", "ep_2", "tp"))
    placed = (
        P(EP, "tp"),
        P(EP, "tp"),
        P(EP, "tp"),
        P(EP, "tp"),
        P("tp", EP),
        P("tp", EP),
        P("tp", EP),
        P("tp"),
        P(EP_TP, None),
        P(),
        P(EP_TP, None),
        P(EP_TP, None),
        P(EP, None, "tp"),
        P(EP, None, "tp"),
        P(EP, "tp", None),
    )
    return jax.shard_map(
        local, mesh=finer, in_specs=placed, out_specs=(P(EP, "tp"), P(EP_TP, None)), check_vma=False
    )
```

profile of v0, /device:TPU:8, one launch (start us, length us, event | category | flops | bytes accessed | tf_op | source)
XLA Modules:
  0.0 352.7 jit_solution(4525034145210452684)
XLA Ops:
  7.3 0.8 add.1943
  8.0 0.7 fusion.67
  8.9 0.5 reduce_window_sum.28
  9.8 1.0 reshape.3327
  11.0 1.0 reshape.3325
  12.4 2.0 fusion.38
  14.4 17.1 %while.25 = (s32[]{:T(128)}, f32[2,256,256]{2,1,0:T(8,128)S(1)}, f32[2,256]{1,0:T(2,128)S(1)}, f32[2]{0:T(128)S(1)}, f32[2]{0:T(128)S(1)}, /*index=5*/f32[4,2,25...) while((s32[]{:T(128)}, f32[2,256,256]{2,1,0:T(8,128)S(1)}, ...), condition=%wide.region_3.4_spmd.clone, body=%wide.region_2.3_spmd.clone.sunk | while | flops 657939 | bytes 2632044 | solution.py:120
  14.4 0.9 bitcast_dynamic-update-slice_fusion.4
  15.5 0.6 bitcast_dynamic-update-slice_fusion.5
  16.1 1.3 dynamic_update_slice.27
  17.4 1.3 dynamic_update_slice.28
  18.7 0.9 bitcast_dynamic-update-slice_fusion.4
  19.7 0.6 bitcast_dynamic-update-slice_fusion.5
  20.4 1.3 dynamic_update_slice.27
  21.7 1.3 dynamic_update_slice.28
  23.0 0.9 bitcast_dynamic-update-slice_fusion.4
  24.0 0.6 bitcast_dynamic-update-slice_fusion.5
  24.7 1.3 dynamic_update_slice.27
  26.0 1.3 dynamic_update_slice.28
  27.3 0.8 bitcast_dynamic-update-slice_fusion.4
  28.3 0.6 bitcast_dynamic-update-slice_fusion.5
  29.0 1.3 dynamic_update_slice.27
  30.3 1.3 dynamic_update_slice.28
  31.6 0.8 maximum_bitcast_fusion
  33.1 0.6 reduce-window.6
  34.4 15.4 %all-gather.13.cloned.1.call-done = f32[2,516,256]{2,1,0:T(8,128)} async-done(((f32[1,516,256]{2,1,0:T(8,128)}), f32[2,516,256]{2,1,0:T(8,128)}) %all-gather.13.cloned.1.call-update) | async-done | bytes 1056784 | tf_op jit(solution)/shard_map/all_gather | solution.py:30
  49.9 0.8 fusion.135
  51.2 0.8 broadcast_bitcast_fusion.11
  52.0 1.5 fusion.34
  53.6 0.8 maximum_bitcast_fusion.1
  54.5 2.4 gather_fusion
  57.0 0.6 gather.9
  58.0 61.6 %all_to_all.26 = bf16[64,5,2048]{2,1,0:T(8,128)(2,1)S(1)} all-to-all(bf16[64,5,2048]{2,1,0:T(8,128)(2,1)S(1)} %broadcast_select_fusion.3), channel_id=1, replica_groups=mesh['ep_0'=8,'ep_1'=4,'ep_2'=2,'tp'=4] {'ep_0','ep_1','ep_2'}, dimensions={0} | all-to-all | bytes 2621440 | tf_op jit(solution)/shard_map/all_to_all | solution.py:221
  119.6 1.4 all_to_all.18
  121.3 0.8 fusion.133
  122.2 0.6 subtract_exponential_fusion.18
  122.9 0.8 broadcast_bitcast_fusion.7
  123.9 2.0 fusion.27
  125.9 0.9 maximum_bitcast_fusion.2
  126.8 49.9 %all-gather.11.cloned.1.call-done = bf16[1280,2048]{1,0:T(8,128)(2,1)} async-done(((bf16[320,2048]{1,0:T(8,128)(2,1)}), bf16[1280,2048]{1,0:T(8,128)(2,1)}) %all-gather.11.cloned.1.call-update) | async-done | bytes 5242896 | tf_op jit(solution)/shard_map/all_gather | solution.py:222
  176.7 9.9 %fusion.11 = f32[1280,896]{1,0:T(8,128)} fusion(bf16[1280,2048]{1,0:T(8,128)(2,1)} %all-gather.11.cloned.1.call-done, bf16[1,2048,896]{2,1,0:T(8,128)(2,1)} %param.29), kind=kOutput, calls=%fused_computation.26 | convolution fusion | flops 4697620480 | bytes 13500416 | tf_op jit(solution)/shard_map/dot_general | solution.py:223
  186.7 17.7 %convolution_convert_fusion = bf16[1280,2048]{1,0:T(8,128)(2,1)} fusion(bf16[1,896,2048]{2,1,0:T(8,128)(2,1)} %param.31, f32[1280,896]{1,0:T(8,128)} %fusion.11, bf16[1280,2048]{1,0:T(8,128)(2,1)} %all-gather.11.cloned.1.call-done, bf16[1,2048,896]{2,1,0:T(8,128)(2,1)} %param.30), kind=kOutput, calls=%fused_computation.22 | convolution fusion | flops 9404743680 | bytes 22413312 | tf_op jit(solution)/shard_map/dot_general | solution.py:227
  204.4 5.2 %all-to-all-start.1 = ((bf16[4,320,2048]{2,1,0:T(8,128)(2,1)}), bf16[4,320,2048]{2,1,0:T(8,128)(2,1)}, u32[]{:S(2)}, u32[]{:S(2)}) async-start(bf16[4,320,2048]{2,1,0:T(8,128)(2,1)} %bitcast.529), calls=%async_computation.1 | async-start | bytes 10485760 | tf_op jit(solution)/shard_map/all_to_all | solution.py:61
  209.8 0.8 reshape.3324
  210.6 0.7 compare_select_fusion.1
  211.6 0.8 copy.148
  212.6 1.0 fusion.134
  213.9 1.4 fusion.132
  215.3 19.0 %all-gather.17.cloned.1.call-done = f32[8,516,256]{2,1,0:T(8,128)} async-done(((f32[1,516,256]{2,1,0:T(8,128)}), f32[8,516,256]{2,1,0:T(8,128)}) %all-gather.17.cloned.1.call-update) | async-done | bytes 4227088 | tf_op jit(solution)/shard_map/all_gather | solution.py:30
  234.3 0.9 fusion.131
  235.9 1.0 add_bitcast_fusion.2
  236.9 32.8 %all-to-all-done.1 = bf16[4,320,2048]{2,1,0:T(8,128)(2,1)} async-done(((bf16[4,320,2048]{2,1,0:T(8,128)(2,1)}), bf16[4,320,2048]{2,1,0:T(8,128)(2,1)}, u32[]{:S(2)}, u32[]{:S(2)}) %all-to-all-start.1) | async-done | bytes 5242912 | tf_op jit(solution)/shard_map/all_to_all | solution.py:61
  269.7 3.6 %reduce_sum.66 = bf16[320,2048]{1,0:T(8,128)(2,1)S(1)} reduce(bf16[4,320,2048]{2,1,0:T(8,128)(2,1)} %all-to-all-done.1, bf16[]{:T(256)} %constant.113.clone.1), dimensions={0}, to_apply=%region_11.12 | reduce | flops 1966080 | bytes 6553602 | tf_op jit(solution)/shard_map/reduce_sum | solution.py:62
  273.3 1.6 all_to_all.20
  275.0 10.7 %all-to-all-start.2 = ((bf16[64,5,2048]{2,1,0:T(8,128)(2,1)}), bf16[64,5,2048]{2,1,0:T(8,128)(2,1)S(1)}, u32[]{:S(2)}, u32[]{:S(2)}) async-start(bf16[64,5,2048]{2,1,0:T(8,128)(2,1)} %all_to_all.20), calls=%async_computation.2 | async-start | bytes 4194304 | tf_op jit(solution)/shard_map/all_to_all | solution.py:231
  286.5 2.8 fusion.130
  289.5 1.4 multiply_add_fusion.1
  291.1 1.5 fusion.20
  293.5 0.9 multiply_convert_fusion.1
  294.4 42.5 %all-to-all-done.2 = bf16[64,5,2048]{2,1,0:T(8,128)(2,1)S(1)} async-done(((bf16[64,5,2048]{2,1,0:T(8,128)(2,1)}), bf16[64,5,2048]{2,1,0:T(8,128)(2,1)S(1)}, u32[]{:S(2)}, u32[]{:S(2)}) %all-to-all-start.2) | async-done | bytes 1310752 | tf_op jit(solution)/shard_map/all_to_all | solution.py:231
  336.9 0.6 all_to_all.22
  337.5 2.4 gather_fusion.1
  339.9 2.4 reshape.3367
  342.2 3.9 %multiply_reduce_fusion = bf16[128,2048]{1,0:T(8,128)(2,1)} fusion(f32[128,2,2048]{2,1,0:T(2,128)S(1)} %reshape.3367, f32[128,2]{1,0:T(8,128)S(1)} %copy.148), kind=kLoop, calls=%fused_computation.30 | loop fusion | flops 786432 | bytes 2622464 | tf_op jit(solution)/shard_map/reduce_sum | solution.py:233
  (233 shorter events, 8.1 us)
Async XLA Ops:
  7.2 42.7 %all-gather.13.cloned.1.call-start = ((), (), s32[]{:S(2)}) async-start(), calls=%async_computation.4 | async-start | bytes 1597440 | tf_op jit(solution)/shard_map/all_gather | solution.py:30
  10.9 3.6 %copy-start.10 = (bf16[4,64,2,256]{3,2,1,0:T(2,128)(2,1)}, bf16[4,64,2,256]{3,2,1,0:T(2,128)(2,1)S(1)}, u32[]{:S(2)}) copy-start(bf16[4,64,2,256]{3,2,1,0:T(2,128)(2,1)S(1)} %reshape.3327) | copy-start | bytes 786436
  12.0 2.4 copy-start.12
  14.4 18.1 %copy-start.54 = (s32[128,2]{0,1:T(2,128)S(1)}, s32[128,2]{0,1:T(2,128)}, u32[]{:S(2)}) copy-start(s32[128,2]{0,1:T(2,128)} %param.27) | copy-start | bytes 3076
  31.5 1.3 copy-start.2
  31.5 2.7 copy-start.17
  32.4 88.8 %all-gather.15.cloned.1.call-start = ((), (), s32[]{:S(2)}) async-start(), calls=%async_computation.5 | async-start | bytes 2662400 | tf_op jit(solution)/shard_map/all_gather | solution.py:30
  50.7 3.7 %copy-start.32 = (f32[2]{0:T(128)}, f32[2]{0:T(128)S(1)}, u32[]{:S(2)}) copy-start(f32[2]{0:T(128)S(1)} %get-tuple-element.244) | copy-start | bytes 28
  50.7 3.8 %copy-start.41 = (f32[2]{0:T(128)}, f32[2]{0:T(128)S(1)}, u32[]{:S(2)}) copy-start(f32[2]{0:T(128)S(1)} %get-tuple-element.245) | copy-start | bytes 28
  50.7 3.8 %copy-start.36 = (f32[2]{0:T(128)}, f32[2]{0:T(128)S(1)}, u32[]{:S(2)}) copy-start(f32[2]{0:T(128)S(1)} %get-tuple-element.324) | copy-start | bytes 28
  50.7 3.8 %copy-start.38 = (f32[2]{0:T(128)}, f32[2]{0:T(128)S(1)}, u32[]{:S(2)}) copy-start(f32[2]{0:T(128)S(1)} %get-tuple-element.325) | copy-start | bytes 28
  50.8 6.2 %copy-start.34 = (f32[2]{0:T(128)}, f32[2]{0:T(128)S(1)}, u32[]{:S(2)}) copy-start(f32[2]{0:T(128)S(1)} %get-tuple-element.299) | copy-start | bytes 28
  54.4 122.3 %all-gather.11.cloned.1.call-start = ((), (), s32[]{:S(2)}) async-start(), calls=%async_computation.3 | async-start | bytes 6553600 | tf_op jit(solution)/shard_map/all_gather | solution.py:222
  121.0 113.3 %all-gather.17.cloned.1.call-start = ((), (), s32[]{:S(2)}) async-start(), calls=%async_computation.6 | async-start | bytes 4792320 | tf_op jit(solution)/shard_map/all_gather | solution.py:30
  122.1 1.7 copy-start.24
  122.1 1.7 copy-start.43
  122.2 1.7 copy-start.46
  122.2 1.7 copy-start.48
  122.2 1.7 copy-start.50
  122.8 1.0 copy-start.26
  122.8 1.1 copy-start.28
  122.8 1.1 copy-start.30
  122.8 1.0 copy-start.18
  122.8 1.0 copy-start.20
  122.9 1.0 copy-start.22
  204.4 5.4 %copy-start.15 = (bf16[256,512]{1,0:T(8,128)(2,1)S(1)}, bf16[256,512]{1,0:T(8,128)(2,1)}, u32[]{:S(2)}) copy-start(bf16[256,512]{1,0:T(8,128)(2,1)} %param.17) | copy-start | bytes 786436
  204.4 8.2 %copy-start.1 = (f32[2,516,256]{2,1,0:T(8,128)S(1)}, f32[2,516,256]{2,1,0:T(8,128)}, u32[]{:S(2)}) copy-start(f32[2,516,256]{2,1,0:T(8,128)} %all-gather.13.cloned.1.call-done) | copy-start | bytes 3170308
  204.4 65.3 %all-to-all-start.1 = ((bf16[4,320,2048]{2,1,0:T(8,128)(2,1)}), bf16[4,320,2048]{2,1,0:T(8,128)(2,1)}, u32[]{:S(2)}, u32[]{:S(2)}) async-start(bf16[4,320,2048]{2,1,0:T(8,128)(2,1)} %bitcast.529), calls=%async_computation.1 | async-start | bytes 10485760 | tf_op jit(solution)/shard_map/all_to_all | solution.py:61
  209.6 4.1 %copy-start = (f32[4,516,256]{2,1,0:T(8,128)S(1)}, f32[4,516,256]{2,1,0:T(8,128)}, u32[]{:S(2)}) copy-start(f32[4,516,256]{2,1,0:T(8,128)} %all-gather.15.cloned.1.call-done) | copy-start | bytes 6340612
  213.7 21.6 %copy-start.40 = (f32[4,2]{1,0:T(4,128)S(1)}, f32[4,2]{1,0:T(4,128)}, u32[]{:S(2)}) copy-start(f32[4,2]{1,0:T(4,128)} %get-tuple-element.81) | copy-start | bytes 100
  213.7 21.7 %copy-start.56 = (f32[4,2]{1,0:T(4,128)S(1)}, f32[4,2]{1,0:T(4,128)}, u32[]{:S(2)}) copy-start(f32[4,2]{1,0:T(4,128)} %get-tuple-element.76) | copy-start | bytes 100
  213.7 21.9 %copy-start.42 = (f32[2]{0:T(128)S(1)}, f32[2]{0:T(128)}, u32[]{:S(2)}) copy-start(f32[2]{0:T(128)} %copy-done.41) | copy-start | bytes 28
  213.7 21.9 %copy-start.44 = (f32[2]{0:T(128)S(1)}, f32[2]{0:T(128)}, u32[]{:S(2)}) copy-start(f32[2]{0:T(128)} %copy-done.43) | copy-start | bytes 28
  213.7 21.9 %copy-start.47 = (f32[2]{0:T(128)S(1)}, f32[2]{0:T(128)}, u32[]{:S(2)}) copy-start(f32[2]{0:T(128)} %copy-done.46) | copy-start | bytes 28
  213.7 21.9 %copy-start.49 = (f32[2]{0:T(128)S(1)}, f32[2]{0:T(128)}, u32[]{:S(2)}) copy-start(f32[2]{0:T(128)} %copy-done.48) | copy-start | bytes 28
  213.7 21.9 %copy-start.51 = (f32[2]{0:T(128)S(1)}, f32[2]{0:T(128)}, u32[]{:S(2)}) copy-start(f32[2]{0:T(128)} %copy-done.50) | copy-start | bytes 28
  213.7 21.9 %copy-start.53 = (f32[2]{0:T(128)S(1)}, f32[2]{0:T(128)}, u32[]{:S(2)}) copy-start(f32[2]{0:T(128)} %copy-done.52) | copy-start | bytes 28
  213.7 21.9 %copy-start.57 = (f32[2]{0:T(128)S(1)}, f32[2]{0:T(128)}, u32[]{:S(2)}) copy-start(f32[2]{0:T(128)} %get-tuple-element.292) | copy-start | bytes 28
  213.7 21.9 %copy-start.58 = (f32[2]{0:T(128)S(1)}, f32[2]{0:T(128)}, u32[]{:S(2)}) copy-start(f32[2]{0:T(128)} %get-tuple-element.293) | copy-start | bytes 28
  213.7 22.0 %copy-start.19 = (f32[2]{0:T(128)S(1)}, f32[2]{0:T(128)}, u32[]{:S(2)}) copy-start(f32[2]{0:T(128)} %copy-done.18) | copy-start | bytes 28
  213.8 22.0 %copy-start.21 = (f32[2]{0:T(128)S(1)}, f32[2]{0:T(128)}, u32[]{:S(2)}) copy-start(f32[2]{0:T(128)} %copy-done.20) | copy-start | bytes 28
  213.8 22.0 %copy-start.23 = (f32[2]{0:T(128)S(1)}, f32[2]{0:T(128)}, u32[]{:S(2)}) copy-start(f32[2]{0:T(128)} %copy-done.22) | copy-start | bytes 28
  213.8 22.0 %copy-start.25 = (f32[2]{0:T(128)S(1)}, f32[2]{0:T(128)}, u32[]{:S(2)}) copy-start(f32[2]{0:T(128)} %copy-done.24) | copy-start | bytes 28
  213.8 22.0 %copy-start.27 = (f32[2]{0:T(128)S(1)}, f32[2]{0:T(128)}, u32[]{:S(2)}) copy-start(f32[2]{0:T(128)} %copy-done.26) | copy-start | bytes 28
  213.8 22.0 %copy-start.29 = (f32[2]{0:T(128)S(1)}, f32[2]{0:T(128)}, u32[]{:S(2)}) copy-start(f32[2]{0:T(128)} %copy-done.28) | copy-start | bytes 28
  213.8 22.0 %copy-start.31 = (f32[2]{0:T(128)S(1)}, f32[2]{0:T(128)}, u32[]{:S(2)}) copy-start(f32[2]{0:T(128)} %copy-done.30) | copy-start | bytes 28
  213.8 22.0 %copy-start.33 = (f32[2]{0:T(128)S(1)}, f32[2]{0:T(128)}, u32[]{:S(2)}) copy-start(f32[2]{0:T(128)} %copy-done.32) | copy-start | bytes 28
  213.8 22.0 %copy-start.35 = (f32[2]{0:T(128)S(1)}, f32[2]{0:T(128)}, u32[]{:S(2)}) copy-start(f32[2]{0:T(128)} %copy-done.34) | copy-start | bytes 28
  213.8 22.0 %copy-start.37 = (f32[2]{0:T(128)S(1)}, f32[2]{0:T(128)}, u32[]{:S(2)}) copy-start(f32[2]{0:T(128)} %copy-done.36) | copy-start | bytes 28
  213.8 22.0 %copy-start.39 = (f32[2]{0:T(128)S(1)}, f32[2]{0:T(128)}, u32[]{:S(2)}) copy-start(f32[2]{0:T(128)} %copy-done.38) | copy-start | bytes 28
  213.9 23.0 %copy-start.45 = (f32[4,2,256]{2,1,0:T(2,128)S(1)}, f32[4,2,256]{2,1,0:T(2,128)}, u32[]{:S(2)}) copy-start(f32[4,2,256]{2,1,0:T(2,128)} %get-tuple-element.83) | copy-start | bytes 24580
  275.0 10.8 %copy-start.14 = (bf16[4,64,2,256]{3,2,1,0:T(2,128)(2,1)S(1)}, bf16[4,64,2,256]{3,2,1,0:T(2,128)(2,1)}, u32[]{:S(2)}) copy-start(bf16[4,64,2,256]{3,2,1,0:T(2,128)(2,1)} %reshape.3324) | copy-start | bytes 786436
  275.0 11.1 %copy-start.13 = (bf16[4,64,2,256]{3,2,1,0:T(2,128)(2,1)S(1)}, bf16[4,64,2,256]{3,2,1,0:T(2,128)(2,1)}, u32[]{:S(2)}) copy-start(bf16[4,64,2,256]{3,2,1,0:T(2,128)(2,1)} %copy-done.12) | copy-start | bytes 786436
  275.0 61.9 %all-to-all-start.2 = ((bf16[64,5,2048]{2,1,0:T(8,128)(2,1)}), bf16[64,5,2048]{2,1,0:T(8,128)(2,1)S(1)}, u32[]{:S(2)}, u32[]{:S(2)}) async-start(bf16[64,5,2048]{2,1,0:T(8,128)(2,1)} %all_to_all.20), calls=%async_computation.2 | async-start | bytes 4194304 | tf_op jit(solution)/shard_map/all_to_all | solution.py:231
  286.4 2.8 copy-start.3
  286.4 2.8 copy-start.4
  286.4 2.8 copy-start.6
  286.4 2.8 copy-start.7
  286.5 2.9 copy-start.8
  286.5 3.1 copy-start.9
  289.5 1.6 copy-start.5
  291.0 1.6 copy-start.11
  292.6 1.0 copy-start.16
  292.6 0.9 copy-start.55
  (1 other events, 0.5 us)
Sparse Core Ops, SparseCore 0:
  32.5 17.2 all-gather.12
  54.5 50.8 all-gather.14
  121.1 55.5 all-gather.10
  178.4 55.8 all-gather.16
where the time goes:
time: 354 us; the launch traced here: 353 us
  waiting for transfers between devices  160 us (45%)
  blocking collectives  61.6 us (17%)
  local copies, waits for them, and re-layouts  37.3 us (11%)
  matrix products  32.3 us (9%)
  other arithmetic  30.3 us (9%)
  starting transfers between devices  16.3 us (5%)
  between operations  15.1 us (4%)
    all_to_all x1, blocking collectives, local(): lax.all_to_all(sendbuf, EP, split_axis=0, concat_axis=0, tiled=True)  61.6 us
    all_gather x1, waiting for transfers between devices, local(): routed_rows = lax.all_gather(arrived, 'tp', axis=0, tiled=True)  49.9 us
    all_to_all x1, waiting for transfers between devices, local(): lax.all_to_all(summed, EP, split_axis=0, concat_axis=0, tiled=True)  42.5 us
    all_gather x3, waiting for transfers between devices, collected_together(): both, at, found = (lax.all_gather(jnp.concatenate(lines), axis), 0, {})  34.5 us
    all_to_all x1, waiting for transfers between devices, sum_at_owner(): blocks = lax.all_to_all(split_up(x, dim, size), axis, 0, 0, tiled=True)  32.8 us
    dot_general x1, matrix products, local(): jnp.dot(hidden, down_matrix, preferred_element_type=jnp.float32)  17.7 us
    all_to_all x1, starting transfers between devices, local(): lax.all_to_all(summed, EP, split_axis=0, concat_axis=0, tiled=True)  10.7 us
    dynamic_update_slice x8, local copies, waits for them, and re-layouts, mix_heads(): device_total, before = lax.scan(fold_step, identity_state, block_terms)  10.3 us
  transfers between devices with their start and end apart: 6, of which 5 were waited for; matrix products, arithmetic and copies ran while one was open for 15% of the time, Pallas kernels for 0%

commit v1 on v0

--- a/solution.py
+++ b/solution.py
@@ -11,6 +11,15 @@
 EP_TP = ("ep_0", "ep_1", "ep_2", "tp")
 EPSILON = 1e-06
 PRECISE = lax.Precision.HIGHEST
+
+
+def draft_turns_on(message, dim_k):
+    p_count = jax.lax.axis_size("tp")
+    windows = []
+    for j0 in tuple(range(message.ndim)):
+        windows.append(p_count if j0 == dim_k else 1)
+    vec_out = jnp.tile(message, windows)
+    return jax.lax.all_to_all(vec_out, "tp", split_axis=dim_k, concat_axis=dim_k, tiled=True)
 
 
 def nothing_yet(x, identity):
@@ -219,7 +228,7 @@
         jnp.zeros((), jnp.bfloat16),
     )
     arrived = lax.all_to_all(sendbuf, EP, split_axis=0, concat_axis=0, tiled=True)
-    routed_rows = lax.all_gather(arrived, "tp", axis=0, tiled=True)
+    routed_rows = draft_turns_on(arrived, 0)
     gate_out = jnp.dot(routed_rows, gate_matrix, preferred_element_type=jnp.float32)
     up_out = jnp.dot(routed_rows, up_matrix, preferred_element_type=jnp.float32)
     hidden = (jax.nn.silu(gate_out) * up_out).astype(jnp.bfloat16)

time: 354 us -> 342 us (0.966)
  blocking collectives: 61.6 us -> 0 us
  waiting for transfers between devices: 160 us -> 192 us
  starting transfers between devices: 16.3 us -> 32.4 us
    all_to_all x0 -> x2, waiting for transfers between devices: none -> 99.6 us  [the longest x1 53.1 us: draft_turns_on(): jax.lax.all_to_all(vec_out, 'tp', split_axis=dim_k, concat_axis=dim_k, ti...]
    all_to_all x1 -> x0, blocking collectives: 61.6 us -> none  [local(): lax.all_to_all(sendbuf, EP, split_axis=0, concat_axis=0, tiled=True)]
    all_gather x1 -> x0, waiting for transfers between devices: 49.9 us -> none  [local(): routed_rows = lax.all_gather(arrived, 'tp', axis=0, tiled=True)]
    all_gather x3, waiting for transfers between devices: 34.5 us -> 0.06 us  [collected_together(): both, at, found = (lax.all_gather(jnp.concatenate(lines), axis), 0, {})]
    all_to_all x1, waiting for transfers between devices: 32.8 us -> 52.5 us  [sum_at_owner(): blocks = lax.all_to_all(split_up(x, dim, size), axis, 0, 0, tiled=True)]
    all_to_all x0 -> x2, starting transfers between devices: none -> 17.2 us  [the longest x1 12.1 us: local(): lax.all_to_all(sendbuf, EP, split_axis=0, concat_axis=0, tiled=True)]
    another operation x1 -> x3, local copies, waits for them, and re-layouts: 0.01 us -> 3.63 us  [the longest x2 3.62 us: draft_turns_on(): vec_out = jnp.tile(message, windows)]
  transfers between devices with their start and end apart: 6 -> 7, of which waited for: 5 -> 4; matrix products, arithmetic and copies ran while one was open for 15% -> 19% of each run, Pallas kernels for 0% -> 0%
where the time goes in v1:
time: 342 us; the launch traced here: 341 us
  waiting for transfers between devices  192 us (56%)
  local copies, waits for them, and re-layouts  37.5 us (11%)
  starting transfers between devices  32.4 us (9%)
  matrix products  32.2 us (9%)
  other arithmetic  31.7 us (9%)
  between operations  15.1 us (4%)
    all_to_all x1, waiting for transfers between devices, draft_turns_on(): jax.lax.all_to_all(vec_out, 'tp', split_axis=dim_k, concat_axis=dim_k, ti...  53.1 us
    all_to_all x1, waiting for transfers between devices, sum_at_owner(): blocks = lax.all_to_all(split_up(x, dim, size), axis, 0, 0, tiled=True)  52.5 us
    all_to_all x1, waiting for transfers between devices, local(): lax.all_to_all(sendbuf, EP, split_axis=0, concat_axis=0, tiled=True)  46.6 us
    all_to_all x1, waiting for transfers between devices, local(): lax.all_to_all(summed, EP, split_axis=0, concat_axis=0, tiled=True)  39.8 us
    dot_general x1, matrix products, local(): jnp.dot(hidden, down_matrix, preferred_element_type=jnp.float32)  17.5 us
    all_to_all x1, starting transfers between devices, local(): lax.all_to_all(sendbuf, EP, split_axis=0, concat_axis=0, tiled=True)  12.1 us
    dynamic_update_slice x8, local copies, waits for them, and re-layouts, mix_heads(): device_total, before = lax.scan(fold_step, identity_state, block_terms)  10.3 us
    dot_general x1, matrix products, local(): jnp.dot(routed_rows, gate_matrix, preferred_element_type=jnp.float32)  9.96 us
  transfers between devices with their start and end apart: 7, of which 4 were waited for; matrix products, arithmetic and copies ran while one was open for 19% of the time, Pallas kernels for 0%

profile of v1, /device:TPU:8, one launch (start us, length us, event | category | flops | bytes accessed | tf_op | source)
XLA Modules:
  0.0 341.0 jit_solution(855151945080780182)
XLA Ops:
  7.3 0.8 add.1943
  8.0 0.7 fusion.67
  9.8 1.0 reshape.3335
  11.0 1.0 reshape.3333
  12.4 2.0 fusion.38
  14.4 17.1 %while.25 = (s32[]{:T(128)}, f32[2,256,256]{2,1,0:T(8,128)S(1)}, f32[2,256]{1,0:T(2,128)S(1)}, f32[2]{0:T(128)S(1)}, f32[2]{0:T(128)S(1)}, /*index=5*/f32[4,2,25...) while((s32[]{:T(128)}, f32[2,256,256]{2,1,0:T(8,128)S(1)}, ...), condition=%wide.region_3.4_spmd.clone, body=%wide.region_2.3_spmd.clone.sunk | while | flops 657939 | bytes 2632044 | solution.py:129
  14.4 0.8 bitcast_dynamic-update-slice_fusion.4
  15.5 0.6 bitcast_dynamic-update-slice_fusion.5
  16.2 1.3 dynamic_update_slice.27
  17.4 1.3 dynamic_update_slice.28
  18.7 0.8 bitcast_dynamic-update-slice_fusion.4
  19.8 0.6 bitcast_dynamic-update-slice_fusion.5
  20.4 1.3 dynamic_update_slice.27
  21.7 1.3 dynamic_update_slice.28
  23.0 0.8 bitcast_dynamic-update-slice_fusion.4
  24.0 0.6 bitcast_dynamic-update-slice_fusion.5
  24.7 1.3 dynamic_update_slice.27
  26.0 1.3 dynamic_update_slice.28
  27.3 0.8 bitcast_dynamic-update-slice_fusion.4
  28.3 0.6 bitcast_dynamic-update-slice_fusion.5
  29.0 1.3 dynamic_update_slice.27
  30.2 1.3 dynamic_update_slice.28
  31.6 0.8 maximum_bitcast_fusion
  33.0 0.6 reduce-window.6
  34.4 2.4 gather_fusion
  37.6 1.6 broadcast_select_fusion.3
  39.2 12.1 %all-to-all-start = ((bf16[64,5,2048]{2,1,0:T(8,128)(2,1)}), bf16[64,5,2048]{2,1,0:T(8,128)(2,1)S(1)}, u32[]{:S(2)}, u32[]{:S(2)}) async-start(bf16[64,5,2048]{2,1,0:T(8,128)(2,1)} %broadcast_select_fusion.3), calls=%async_computation | async-start | bytes 4194304 | tf_op jit(solution)/shard_map/all_to_all | solution.py:230
  51.3 0.8 fusion.135
  52.7 0.8 broadcast_bitcast_fusion.11
  53.5 1.5 fusion.34
  55.1 0.8 maximum_bitcast_fusion.1
  56.0 46.6 %all-to-all-done = bf16[64,5,2048]{2,1,0:T(8,128)(2,1)S(1)} async-done(((bf16[64,5,2048]{2,1,0:T(8,128)(2,1)}), bf16[64,5,2048]{2,1,0:T(8,128)(2,1)S(1)}, u32[]{:S(2)}, u32[]{:S(2)}) %all-to-all-start) | async-done | bytes 1310752 | tf_op jit(solution)/shard_map/all_to_all | solution.py:230
  102.5 0.6 tile.4
  103.1 3.1 tile.10
  106.2 5.1 %all-to-all-start.1 = ((bf16[4,320,2048]{2,1,0:T(8,128)(2,1)}), bf16[4,320,2048]{2,1,0:T(8,128)(2,1)}, u32[]{:S(2)}, u32[]{:S(2)}) async-start(bf16[4,320,2048]{2,1,0:T(8,128)(2,1)} %tile.10), calls=%async_computation.1 | async-start | bytes 10485760 | tf_op jit(solution)/shard_map/all_to_all | solution.py:22
  111.5 0.8 fusion.133
  112.4 0.6 subtract_exponential_fusion.18
  113.1 0.8 broadcast_bitcast_fusion.7
  114.1 2.0 fusion.27
  116.1 0.9 maximum_bitcast_fusion.2
  117.0 53.1 %all-to-all-done.1 = bf16[4,320,2048]{2,1,0:T(8,128)(2,1)} async-done(((bf16[4,320,2048]{2,1,0:T(8,128)(2,1)}), bf16[4,320,2048]{2,1,0:T(8,128)(2,1)}, u32[]{:S(2)}, u32[]{:S(2)}) %all-to-all-start.1) | async-done | bytes 5242912 | tf_op jit(solution)/shard_map/all_to_all | solution.py:22
  170.1 10.0 %fusion.11 = f32[1280,896]{1,0:T(8,128)} fusion(bf16[1280,2048]{1,0:T(8,128)(2,1)} %bitcast.87, bf16[1,2048,896]{2,1,0:T(8,128)(2,1)} %param.29), kind=kOutput, calls=%fused_computation.26 | convolution fusion | flops 4697620480 | bytes 13500416 | tf_op jit(solution)/shard_map/dot_general | solution.py:232
  180.1 17.5 %convolution_convert_fusion = bf16[1280,2048]{1,0:T(8,128)(2,1)} fusion(bf16[1,896,2048]{2,1,0:T(8,128)(2,1)} %param.31, f32[1280,896]{1,0:T(8,128)} %fusion.11, bf16[1280,2048]{1,0:T(8,128)(2,1)} %bitcast.87, bf16[1,2048,896]{2,1,0:T(8,128)(2,1)} %param.30), kind=kOutput, calls=%fused_computation.22 | convolution fusion | flops 9404743680 | bytes 22413312 | tf_op jit(solution)/shard_map/dot_general | solution.py:236
  197.6 5.2 %all-to-all-start.2 = ((bf16[4,320,2048]{2,1,0:T(8,128)(2,1)}), bf16[4,320,2048]{2,1,0:T(8,128)(2,1)}, u32[]{:S(2)}, u32[]{:S(2)}) async-start(bf16[4,320,2048]{2,1,0:T(8,128)(2,1)} %bitcast.530), calls=%async_computation.2 | async-start | bytes 10485760 | tf_op jit(solution)/shard_map/all_to_all | solution.py:70
  203.0 0.8 reshape.3332
  203.8 0.7 compare_select_fusion.1
  204.8 0.8 copy.148
  205.8 1.0 fusion.134
  206.9 1.4 fusion.132
  208.3 52.5 %all-to-all-done.2 = bf16[4,320,2048]{2,1,0:T(8,128)(2,1)} async-done(((bf16[4,320,2048]{2,1,0:T(8,128)(2,1)}), bf16[4,320,2048]{2,1,0:T(8,128)(2,1)}, u32[]{:S(2)}, u32[]{:S(2)}) %all-to-all-start.2) | async-done | bytes 5242912 | tf_op jit(solution)/shard_map/all_to_all | solution.py:70
  260.8 3.6 %reduce_sum.66 = bf16[320,2048]{1,0:T(8,128)(2,1)S(1)} reduce(bf16[4,320,2048]{2,1,0:T(8,128)(2,1)} %all-to-all-done.2, bf16[]{:T(256)} %constant.113.clone.1), dimensions={0}, to_apply=%region_11.12 | reduce | flops 1966080 | bytes 6553602 | tf_op jit(solution)/shard_map/reduce_sum | solution.py:71
  264.4 1.6 all_to_all.25
  266.3 9.7 %all-to-all-start.3 = ((bf16[64,5,2048]{2,1,0:T(8,128)(2,1)}), bf16[64,5,2048]{2,1,0:T(8,128)(2,1)S(1)}, u32[]{:S(2)}, u32[]{:S(2)}) async-start(bf16[64,5,2048]{2,1,0:T(8,128)(2,1)} %all_to_all.25), calls=%async_computation.3 | async-start | bytes 4194304 | tf_op jit(solution)/shard_map/all_to_all | solution.py:240
  276.1 0.9 fusion.131
  277.6 1.0 add_bitcast_fusion.2
  279.5 2.8 fusion.130
  282.6 1.4 multiply_add_fusion.1
  284.2 1.5 fusion.20
  286.6 0.9 multiply_convert_fusion.1
  287.4 39.8 %all-to-all-done.3 = bf16[64,5,2048]{2,1,0:T(8,128)(2,1)S(1)} async-done(((bf16[64,5,2048]{2,1,0:T(8,128)(2,1)}), bf16[64,5,2048]{2,1,0:T(8,128)(2,1)S(1)}, u32[]{:S(2)}, u32[]{:S(2)}) %all-to-all-start.3) | async-done | bytes 1310752 | tf_op jit(solution)/shard_map/all_to_all | solution.py:240
  327.3 0.6 all_to_all.27
  327.8 1.4 gather_fusion.1
  329.2 1.3 reshape.3375
  330.5 3.9 %multiply_reduce_fusion = bf16[128,2048]{1,0:T(8,128)(2,1)} fusion(f32[128,2,2048]{2,1,0:T(2,128)S(1)} %reshape.3375, f32[128,2]{1,0:T(8,128)S(1)} %copy.148), kind=kLoop, calls=%fused_computation.30 | loop fusion | flops 786432 | bytes 2622464 | tf_op jit(solution)/shard_map/reduce_sum | solution.py:242
  (234 shorter events, 8.9 us)
Async XLA Ops:
  7.2 44.2 %all-gather.10.cloned.1.call-start = ((), (), s32[]{:S(2)}) async-start(), calls=%async_computation.4 | async-start | bytes 1597440 | tf_op jit(solution)/shard_map/all_gather | solution.py:39
  10.9 3.6 %copy-start.10 = (bf16[4,64,2,256]{3,2,1,0:T(2,128)(2,1)}, bf16[4,64,2,256]{3,2,1,0:T(2,128)(2,1)S(1)}, u32[]{:S(2)}) copy-start(bf16[4,64,2,256]{3,2,1,0:T(2,128)(2,1)S(1)} %reshape.3335) | copy-start | bytes 786436
  12.0 2.4 copy-start.12
  14.4 18.0 %copy-start.54 = (s32[128,2]{0,1:T(2,128)S(1)}, s32[128,2]{0,1:T(2,128)}, u32[]{:S(2)}) copy-start(s32[128,2]{0,1:T(2,128)} %param.27) | copy-start | bytes 3076
  31.5 1.3 copy-start.2
  31.5 2.6 copy-start.17
  39.2 63.3 %all-to-all-start = ((bf16[64,5,2048]{2,1,0:T(8,128)(2,1)}), bf16[64,5,2048]{2,1,0:T(8,128)(2,1)S(1)}, u32[]{:S(2)}, u32[]{:S(2)}) async-start(bf16[64,5,2048]{2,1,0:T(8,128)(2,1)} %broadcast_select_fusion.3), calls=%async_computation | async-start | bytes 4194304 | tf_op jit(solution)/shard_map/all_to_all | solution.py:230
  51.3 60.2 %all-gather.12.cloned.1.call-start = ((), (), s32[]{:S(2)}) async-start(), calls=%async_computation.5 | async-start | bytes 2662400 | tf_op jit(solution)/shard_map/all_gather | solution.py:39
  52.2 1.3 copy-start.41
  52.2 50.9 %copy-start.32 = (f32[2]{0:T(128)}, f32[2]{0:T(128)S(1)}, u32[]{:S(2)}) copy-start(f32[2]{0:T(128)S(1)} %get-tuple-element.244) | copy-start | bytes 28
  52.2 3.7 %copy-start.36 = (f32[2]{0:T(128)}, f32[2]{0:T(128)S(1)}, u32[]{:S(2)}) copy-start(f32[2]{0:T(128)S(1)} %get-tuple-element.324) | copy-start | bytes 28
  52.2 3.7 %copy-start.38 = (f32[2]{0:T(128)}, f32[2]{0:T(128)S(1)}, u32[]{:S(2)}) copy-start(f32[2]{0:T(128)S(1)} %get-tuple-element.325) | copy-start | bytes 28
  52.2 50.9 %copy-start.34 = (f32[2]{0:T(128)}, f32[2]{0:T(128)S(1)}, u32[]{:S(2)}) copy-start(f32[2]{0:T(128)S(1)} %get-tuple-element.299) | copy-start | bytes 28
  106.2 63.9 %all-to-all-start.1 = ((bf16[4,320,2048]{2,1,0:T(8,128)(2,1)}), bf16[4,320,2048]{2,1,0:T(8,128)(2,1)}, u32[]{:S(2)}, u32[]{:S(2)}) async-start(bf16[4,320,2048]{2,1,0:T(8,128)(2,1)} %tile.10), calls=%async_computation.1 | async-start | bytes 10485760 | tf_op jit(solution)/shard_map/all_to_all | solution.py:22
  111.2 164.8 %all-gather.14.cloned.1.call-start = ((), (), s32[]{:S(2)}) async-start(), calls=%async_computation.6 | async-start | bytes 4792320 | tf_op jit(solution)/shard_map/all_gather | solution.py:39
  112.4 1.6 copy-start.24
  112.4 1.6 copy-start.43
  112.4 1.6 copy-start.46
  112.4 1.6 copy-start.48
  112.4 1.6 copy-start.50
  113.0 1.0 copy-start.26
  113.0 1.1 copy-start.28
  113.0 1.1 copy-start.30
  113.1 1.0 copy-start.18
  113.1 1.0 copy-start.20
  113.1 1.0 copy-start.22
  197.6 5.4 %copy-start.15 = (bf16[256,512]{1,0:T(8,128)(2,1)S(1)}, bf16[256,512]{1,0:T(8,128)(2,1)}, u32[]{:S(2)}) copy-start(bf16[256,512]{1,0:T(8,128)(2,1)} %param.17) | copy-start | bytes 786436
  197.6 8.2 %copy-start.1 = (f32[2,516,256]{2,1,0:T(8,128)S(1)}, f32[2,516,256]{2,1,0:T(8,128)}, u32[]{:S(2)}) copy-start(f32[2,516,256]{2,1,0:T(8,128)} %all-gather.10.cloned.1.call-done) | copy-start | bytes 3170308
  197.6 63.2 %all-to-all-start.2 = ((bf16[4,320,2048]{2,1,0:T(8,128)(2,1)}), bf16[4,320,2048]{2,1,0:T(8,128)(2,1)}, u32[]{:S(2)}, u32[]{:S(2)}) async-start(bf16[4,320,2048]{2,1,0:T(8,128)(2,1)} %bitcast.530), calls=%async_computation.2 | async-start | bytes 10485760 | tf_op jit(solution)/shard_map/all_to_all | solution.py:70
  202.8 4.0 %copy-start = (f32[4,516,256]{2,1,0:T(8,128)S(1)}, f32[4,516,256]{2,1,0:T(8,128)}, u32[]{:S(2)}) copy-start(f32[4,516,256]{2,1,0:T(8,128)} %all-gather.12.cloned.1.call-done) | copy-start | bytes 6340612
  266.1 11.0 %copy-start.40 = (f32[4,2]{1,0:T(4,128)S(1)}, f32[4,2]{1,0:T(4,128)}, u32[]{:S(2)}) copy-start(f32[4,2]{1,0:T(4,128)} %get-tuple-element.81) | copy-start | bytes 100
  266.1 11.0 %copy-start.56 = (f32[4,2]{1,0:T(4,128)S(1)}, f32[4,2]{1,0:T(4,128)}, u32[]{:S(2)}) copy-start(f32[4,2]{1,0:T(4,128)} %get-tuple-element.76) | copy-start | bytes 100
  266.1 11.2 %copy-start.42 = (f32[2]{0:T(128)S(1)}, f32[2]{0:T(128)}, u32[]{:S(2)}) copy-start(f32[2]{0:T(128)} %copy-done.41) | copy-start | bytes 28
  266.1 11.2 %copy-start.44 = (f32[2]{0:T(128)S(1)}, f32[2]{0:T(128)}, u32[]{:S(2)}) copy-start(f32[2]{0:T(128)} %copy-done.43) | copy-start | bytes 28
  266.1 11.2 %copy-start.47 = (f32[2]{0:T(128)S(1)}, f32[2]{0:T(128)}, u32[]{:S(2)}) copy-start(f32[2]{0:T(128)} %copy-done.46) | copy-start | bytes 28
  266.1 11.2 %copy-start.49 = (f32[2]{0:T(128)S(1)}, f32[2]{0:T(128)}, u32[]{:S(2)}) copy-start(f32[2]{0:T(128)} %copy-done.48) | copy-start | bytes 28
  266.1 11.2 %copy-start.51 = (f32[2]{0:T(128)S(1)}, f32[2]{0:T(128)}, u32[]{:S(2)}) copy-start(f32[2]{0:T(128)} %copy-done.50) | copy-start | bytes 28
  266.1 11.2 %copy-start.53 = (f32[2]{0:T(128)S(1)}, f32[2]{0:T(128)}, u32[]{:S(2)}) copy-start(f32[2]{0:T(128)} %copy-done.52) | copy-start | bytes 28
  266.1 11.2 %copy-start.57 = (f32[2]{0:T(128)S(1)}, f32[2]{0:T(128)}, u32[]{:S(2)}) copy-start(f32[2]{0:T(128)} %get-tuple-element.292) | copy-start | bytes 28
  266.1 11.2 %copy-start.58 = (f32[2]{0:T(128)S(1)}, f32[2]{0:T(128)}, u32[]{:S(2)}) copy-start(f32[2]{0:T(128)} %get-tuple-element.293) | copy-start | bytes 28
  266.1 11.3 %copy-start.19 = (f32[2]{0:T(128)S(1)}, f32[2]{0:T(128)}, u32[]{:S(2)}) copy-start(f32[2]{0:T(128)} %copy-done.18) | copy-start | bytes 28
  266.2 11.3 %copy-start.21 = (f32[2]{0:T(128)S(1)}, f32[2]{0:T(128)}, u32[]{:S(2)}) copy-start(f32[2]{0:T(128)} %copy-done.20) | copy-start | bytes 28
  266.2 11.3 %copy-start.23 = (f32[2]{0:T(128)S(1)}, f32[2]{0:T(128)}, u32[]{:S(2)}) copy-start(f32[2]{0:T(128)} %copy-done.22) | copy-start | bytes 28
  266.2 11.3 %copy-start.25 = (f32[2]{0:T(128)S(1)}, f32[2]{0:T(128)}, u32[]{:S(2)}) copy-start(f32[2]{0:T(128)} %copy-done.24) | copy-start | bytes 28
  266.2 11.3 %copy-start.27 = (f32[2]{0:T(128)S(1)}, f32[2]{0:T(128)}, u32[]{:S(2)}) copy-start(f32[2]{0:T(128)} %copy-done.26) | copy-start | bytes 28
  266.2 11.3 %copy-start.29 = (f32[2]{0:T(128)S(1)}, f32[2]{0:T(128)}, u32[]{:S(2)}) copy-start(f32[2]{0:T(128)} %copy-done.28) | copy-start | bytes 28
  266.2 11.3 %copy-start.31 = (f32[2]{0:T(128)S(1)}, f32[2]{0:T(128)}, u32[]{:S(2)}) copy-start(f32[2]{0:T(128)} %copy-done.30) | copy-start | bytes 28
  266.2 11.3 %copy-start.33 = (f32[2]{0:T(128)S(1)}, f32[2]{0:T(128)}, u32[]{:S(2)}) copy-start(f32[2]{0:T(128)} %copy-done.32) | copy-start | bytes 28
  266.2 11.3 %copy-start.35 = (f32[2]{0:T(128)S(1)}, f32[2]{0:T(128)}, u32[]{:S(2)}) copy-start(f32[2]{0:T(128)} %copy-done.34) | copy-start | bytes 28
  266.2 11.3 %copy-start.37 = (f32[2]{0:T(128)S(1)}, f32[2]{0:T(128)}, u32[]{:S(2)}) copy-start(f32[2]{0:T(128)} %copy-done.36) | copy-start | bytes 28
  266.2 11.3 %copy-start.39 = (f32[2]{0:T(128)S(1)}, f32[2]{0:T(128)}, u32[]{:S(2)}) copy-start(f32[2]{0:T(128)} %copy-done.38) | copy-start | bytes 28
  266.3 12.4 %copy-start.45 = (f32[4,2,256]{2,1,0:T(2,128)S(1)}, f32[4,2,256]{2,1,0:T(2,128)}, u32[]{:S(2)}) copy-start(f32[4,2,256]{2,1,0:T(2,128)} %get-tuple-element.83) | copy-start | bytes 24580
  266.3 12.5 %copy-start.14 = (bf16[4,64,2,256]{3,2,1,0:T(2,128)(2,1)S(1)}, bf16[4,64,2,256]{3,2,1,0:T(2,128)(2,1)}, u32[]{:S(2)}) copy-start(bf16[4,64,2,256]{3,2,1,0:T(2,128)(2,1)} %reshape.3332) | copy-start | bytes 786436
  266.3 12.8 %copy-start.13 = (bf16[4,64,2,256]{3,2,1,0:T(2,128)(2,1)S(1)}, bf16[4,64,2,256]{3,2,1,0:T(2,128)(2,1)}, u32[]{:S(2)}) copy-start(bf16[4,64,2,256]{3,2,1,0:T(2,128)(2,1)} %copy-done.12) | copy-start | bytes 786436
  266.3 61.0 %all-to-all-start.3 = ((bf16[64,5,2048]{2,1,0:T(8,128)(2,1)}), bf16[64,5,2048]{2,1,0:T(8,128)(2,1)S(1)}, u32[]{:S(2)}, u32[]{:S(2)}) async-start(bf16[64,5,2048]{2,1,0:T(8,128)(2,1)} %all_to_all.25), calls=%async_computation.3 | async-start | bytes 4194304 | tf_op jit(solution)/shard_map/all_to_all | solution.py:240
  279.5 2.8 copy-start.3
  279.5 2.8 copy-start.4
  279.5 2.8 copy-start.6
  279.5 2.8 copy-start.7
  279.5 2.9 copy-start.8
  279.5 3.1 copy-start.9
  282.6 1.6 copy-start.5
  284.0 1.6 copy-start.11
  285.6 1.0 copy-start.16
  (2 other events, 1.5 us)
Sparse Core Ops, SparseCore 0:
  32.5 17.2 all-gather.9
  56.1 46.2 all-gather.11
  117.2 51.7 all-gather.13
